TPU v7x, 32 devices: a whole 2x2x4 slice. The times are simulated.
32 devices in a mesh: fs: 4 (over z), rep: 4 (over y, x), tp: 2 (over core).
Axes of the slice: x: 2, y: 2, z: 4, core: 2. Of those that a mesh axis runs over, the one named last changes fastest.
Arguments:
- first_mix: bfloat16 [12288, 2048], P(('fs', 'rep'), 'tp'), may hold values from -6 to 6
- second_mix: bfloat16 [12288, 2048], P(('fs', 'rep'), 'tp'), may hold values from -6 to 6
- lambda_head: float32 [8], P('tp'), may hold values from 0.3 to 0.8
- head_gain: float32 [256], replicated, may hold values from 0.1 to 1.9
- out_cotangent: bfloat16 [12288, 2048], P(('fs', 'rep')), may hold values from -0.053955078 to 0.053955078
- basis: bfloat16 [2048, 256], P('tp'), may hold values from -0.125 to 0.125
- weight: float32 [2048, 2048], P('tp', 'fs'), may hold values from -3 to 3
- first_moment: float32 [2048, 256], P('fs', 'tp'), may hold values from -4.5 to 4.5
- second_moment: float32 [2048, 256], P('fs', 'tp'), may hold values from 0.05 to 0.5
Outputs:
- weight_new: float32 [2048, 2048], P('tp', 'fs')
- weight_copy: bfloat16 [2048, 2048], P('tp')
- step_out: float32 [2048, 2048], P('tp', 'fs')
- first_new: float32 [2048, 256], P('fs', 'tp')
- second_new: float32 [2048, 256], P('fs', 'tp')
All inputs are finite; a program needn't handle non-finite values.
Results may differ from a plain program's by a relative error of at most 0.0075.
Values may be sent and summed in bfloat16 or wider, within the bound.
A program may use at most 64 MiB of HBM per device.

v0:
```python
import jax
import jax.numpy as jnp
from jax import lax
from jax.sharding import PartitionSpec as P

out_scale = 0.8
beta_first = 0.9
beta_second = 0.95


def head_output(first_piece, second_piece, lambdas, head_gain):
    token_count = first_piece.shape[0]
    head_width = head_gain.shape[0]
    head_count = lambdas.shape[0] // head_width
    mixture = first_piece.astype(jnp.float32) - lambdas[None, :] * second_piece.astype(jnp.float32)
    grouped = mixture.reshape(token_count, head_count, head_width)
    inverse = lax.rsqrt(jnp.mean(grouped * grouped, axis=-1, keepdims=True) + 1e-06)
    normed = grouped * inverse * head_gain[None, None, :] * out_scale
    return normed.reshape(token_count, head_count * head_width).astype(jnp.bfloat16)


def split_product(narrow, wide, numbers):
    upper = wide.astype(jnp.bfloat16)
    lower = (wide - upper.astype(jnp.float32)).astype(jnp.bfloat16)
    return lax.dot_general(
        narrow, upper, numbers, preferred_element_type=jnp.float32
    ) + lax.dot_general(narrow, lower, numbers, preferred_element_type=jnp.float32)


def body(
    first_mix,
    second_mix,
    lambda_head,
    head_gain,
    out_cotangent,
    basis,
    weight,
    first_moment,
    second_moment,
):
    lambdas = jnp.repeat(lambda_head, head_gain.shape[0])
    head_out = head_output(first_mix, second_mix, lambdas, head_gain)
    reduced = jnp.dot(head_out, basis, preferred_element_type=jnp.float32)
    proj_rows = lax.psum_scatter(
        split_product(out_cotangent, reduced, (((0,), (0,)), ((), ()))),
        "fs",
        scatter_dimension=0,
        tiled=True,
    )
    proj_rows = lax.psum_scatter(proj_rows, "tp", scatter_dimension=1, tiled=True)
    projected = lax.psum(proj_rows, "rep")
    first_new = beta_first * first_moment + (1.0 - beta_first) * projected
    second_new = beta_second * second_moment + (1.0 - beta_second) * projected * projected
    direction = first_new / (jnp.sqrt(second_new) + 1e-08)
    energy = lax.psum(jnp.sum(direction * direction), ("fs", "tp"))
    entries = direction.shape[0] * direction.shape[1] * lax.axis_size("fs") * lax.axis_size("tp")
    spread = jnp.sqrt(energy / entries)
    full_direction = lax.all_gather(direction, "tp", axis=1, tiled=True)
    step_out = split_product(basis, full_direction, (((1,), (1,)), ((), ()))) * (
        -1.0 / (spread + 1e-06)
    )
    weight_new = weight + step_out
    weight_copy = lax.all_gather(weight_new.astype(jnp.bfloat16), "fs", axis=1, tiled=True)
    return (weight_new, weight_copy, step_out, first_new, second_new)


def solution(mesh):
    return jax.shard_map(
        body,
        mesh=mesh,
        in_specs=(
            P(("fs", "rep"), "tp"),
            P(("fs", "rep"), "tp"),
            P("tp"),
            P(),
            P(("fs", "rep"), None),
            P("tp", None),
            P("tp", "fs"),
            P("fs", "tp"),
            P("fs", "tp"),
        ),
        out_specs=(P("tp", "fs"), P("tp", None), P("tp", "fs"), P("fs", "tp"), P("fs", "tp")),
        check_vma=False,
    )
```

profile of v0, /device:TPU:0, one launch (start us, length us, event | category | flops | bytes accessed | tf_op | source)
XLA Modules:
  0.0 254.0 jit_solution(11689265764747644795)
XLA Ops:
  7.2 0.9 broadcast_bitcast_fusion.1
  8.8 4.2 %fusion = f32[768,1024]{1,0:T(8,128)} fusion(bf16[768,1024]{1,0:T(8,128)(2,1)} %param.10, bf16[768,1024]{1,0:T(8,128)(2,1)} %param.9, f32[1024]{0:T(1024)S(1)} %bitcast.19), kind=kLoop, calls=%fused_computation.2 | loop fusion | flops 3932160 | bytes 6295552 | tf_op jit(solution)/shard_map/mul | solution.py:17
  13.0 5.2 %mul.92 = f32[768,4,256]{2,1,0:T(4,128)} reshape(f32[768,1024]{1,0:T(8,128)} %fusion) | data formatting | bytes 6291456 | tf_op jit(solution)/shard_map/mul | solution.py:17
  18.2 2.8 %reduce_sum.18 = f32[768,4]{1,0:T(8,128)S(1)} reduce(f32[768,4,256]{2,1,0:T(4,128)} %mul.92, f32[]{:T(128)} %constant.2.clone.1), dimensions={2}, to_apply=%region_0.0 | reduce | flops 783360 | bytes 3158020 | tf_op jit(solution)/shard_map/reduce_sum | solution.py:17
  21.1 1.0 mul.93
  24.0 0.9 fusion.2
  25.0 1.0 fusion.5
  26.0 2.4 fusion.1
  28.5 46.5 %reduce-scatter.3.cloned.1.call-done = f32[512,256]{0,1:T(8,128)} async-done(((f32[2048,256]{0,1:T(8,128)}), f32[512,256]{0,1:T(8,128)}) %reduce-scatter.3.cloned.1.call-update) | async-done | bytes 524304 | tf_op jit(solution)/shard_map/reduce_scatter | solution.py:44
  75.0 9.3 %reduce-scatter.5.cloned.1.call-done = f32[512,128]{0,1:T(8,128)} async-done(((f32[512,256]{0,1:T(8,128)}), f32[512,128]{0,1:T(8,128)}) %reduce-scatter.5.cloned.1.call-update) | async-done | bytes 262160 | tf_op jit(solution)/shard_map/reduce_scatter | solution.py:50
  84.4 0.8 copy.31
  85.2 1.8 copy.34
  87.0 2.9 %copy.35 = f32[1024,512]{0,1:T(8,128)} copy(f32[1024,512]{1,0:T(8,128)} %param.15) | data formatting | bytes 4194304 | tf_op args[6]
  89.9 41.6 %all-reduce.2.cloned.1.call-done = f32[512,128]{0,1:T(8,128)} async-done(((f32[512,128]{0,1:T(8,128)}), f32[512,128]{0,1:T(8,128)}) %all-reduce.2.cloned.1.call-update) | async-done | bytes 262160 | tf_op jit(solution)/shard_map/psum | solution.py:51
  131.5 2.6 %multiply_reduce_fusion = (f32[]{:T(128)}, f32[512,128]{0,1:T(8,128)S(1)}, f32[512,128]{0,1:T(8,128)}, f32[512,128]{0,1:T(8,128)}) fusion(f32[512,128]{0,1:T(8,128)} %all-reduce.2.cloned.1.call-done, f32[512,128]{0,1:T(8,128)} %copy.34, f32[512,128]{0,1:T(8,128)} %copy.31), kind=kLoop, calls=%fused_computation.12 | loop fusion | flops 720895 | bytes 1572868 | tf_op jit(solution)/shard_map/reduce_sum | solution.py:55
  134.1 16.5 %psum.15 = f32[]{:T(128)} all-reduce(f32[]{:T(128)} %get-tuple-element.22), channel_id=1, replica_groups=mesh['fs'=4,'rep'=4,'tp'=2] {'fs','tp'}, use_global_device_ids=true, to_apply=%region_5.0 | all-reduce | flops 1 | bytes 8 | tf_op jit(solution)/shard_map/psum | solution.py:55
  151.3 2.2 all_gather.6
  154.3 2.8 %fusion.8 = f32[512,1024]{1,0:T(8,128)} fusion(bf16[1024,256]{1,0:T(8,128)(2,1)} %param.14, f32[512,256]{0,1:T(8,128)S(1)} %all_gather.6), kind=kOutput, calls=%fused_computation.19 | convolution fusion | flops 268566528 | bytes 3145728 | tf_op jit(solution)/shard_map/dot_general | solution.py:25
  157.2 5.7 %fusion.11 = (bf16[1024,512]{0,1:T(8,128)(2,1)}, f32[1024,512]{0,1:T(8,128)}, f32[1024,512]{0,1:T(8,128)}) fusion(f32[1024,512]{0,1:T(8,128)} %copy.35, f32[]{:T(128)S(6)} %div.19, f32[512,1024]{1,0:T(8,128)} %fusion.8, bf16[1024,256]{1,0:T(8,128)(2,1)} %param.14, f32[512,256]{0,1:T(8,128)} %copy-done.4), kind=kOutput, calls=%fused_computation.24 | convolution fusion | flops 271056896 | bytes 10485764 | tf_op jit(solution)/shard_map/dot_general | solution.py:27
  162.9 1.8 copy.40
  165.5 3.0 %copy.36 = f32[1024,512]{1,0:T(8,128)} copy(f32[1024,512]{0,1:T(8,128)} %get-tuple-element.21) | data formatting | bytes 4194304
  168.5 3.0 %copy.38 = f32[1024,512]{1,0:T(8,128)} copy(f32[1024,512]{0,1:T(8,128)} %get-tuple-element.26) | data formatting | bytes 4194304
  171.5 69.5 %all-gather.2.cloned.1.call-done = bf16[1024,2048]{0,1:T(8,128)(2,1)} async-done(((bf16[1024,512]{0,1:T(8,128)(2,1)}), bf16[1024,2048]{0,1:T(8,128)(2,1)}) %all-gather.2.cloned.1.call-update) | async-done | bytes 4194320 | tf_op jit(solution)/shard_map/all_gather | solution.py:63
  241.0 6.4 %copy.37 = bf16[1024,2048]{1,0:T(8,128)(2,1)} copy(bf16[1024,2048]{0,1:T(8,128)(2,1)} %all-gather.2.cloned.1.call-done) | data formatting | bytes 8388608
  (28 shorter events, 4.6 us)
Async XLA Ops:
  7.2 17.8 %copy-start = (bf16[768,2048]{1,0:T(8,128)(2,1)S(1)}, bf16[768,2048]{1,0:T(8,128)(2,1)}, u32[]{:S(2)}) copy-start(bf16[768,2048]{1,0:T(8,128)(2,1)} %param.13) | copy-start | bytes 9437188
  7.2 67.7 %reduce-scatter.3.cloned.1.call-start = ((), (), s32[]{:S(2)}) async-start(), calls=%async_computation.2 | async-start | bytes 2621440 | tf_op jit(solution)/shard_map/reduce_scatter | solution.py:44
  22.0 1.4 copy-start.1
  22.1 1.9 copy-start.2
  22.1 2.0 copy-start.3
  26.0 58.4 %copy-start.6 = (f32[512,128]{1,0:T(8,128)S(1)}, f32[512,128]{1,0:T(8,128)}, u32[]{:S(2)}) copy-start(f32[512,128]{1,0:T(8,128)} %param.16) | copy-start | bytes 786436
  28.4 55.9 %reduce-scatter.5.cloned.1.call-start = ((), (), s32[]{:S(2)}) async-start(), calls=%async_computation.3 | async-start | bytes 786432 | tf_op jit(solution)/shard_map/reduce_scatter | solution.py:50
  74.9 56.5 %all-reduce.2.cloned.1.call-start = ((), (), s32[]{:S(2)}) async-start(), calls=%async_computation.4 | async-start | bytes 524288 | tf_op jit(solution)/shard_map/psum | solution.py:51
  84.4 156.6 %all-gather.2.cloned.1.call-start = ((), (), s32[]{:S(2)}) async-start(), calls=%async_computation.5 | async-start | bytes 5242880 | tf_op jit(solution)/shard_map/all_gather | solution.py:63
  153.5 0.8 copy-start.4
  157.2 7.5 %copy-start.5 = (f32[512,128]{0,1:T(8,128)S(1)}, f32[512,128]{0,1:T(8,128)}, u32[]{:S(2)}) copy-start(f32[512,128]{0,1:T(8,128)} %get-tuple-element.25) | copy-start | bytes 786436
Sparse Core Ops, SparseCore 0:
  28.5 46.3 reduce-scatter.2
  77.2 7.1 reduce-scatter.4
  87.3 44.1 all-reduce.1
  163.0 77.9 all-gather.1
where the time goes:
time: 255 us; the launch traced here: 254 us
  waiting for transfers between devices  167 us (65%)
  local copies, waits for them, and re-layouts  31 us (12%)
  blocking collectives  18.7 us (7%)
  between operations  14.6 us (6%)
  matrix products  12.8 us (5%)
  other arithmetic  9.72 us (4%)
    all_gather x1, waiting for transfers between devices, body(): lax.all_gather(weight_new.astype(jnp.bfloat16), 'fs', axis=1, tiled=True)  69.5 us
    reduce_scatter x1, waiting for transfers between devices, body(): lax.psum_scatter(split_product(out_cotangent, reduced, (((0,), (0,)), (()...  46.5 us
    psum x1, waiting for transfers between devices, body(): projected = lax.psum(proj_rows, 'rep')  41.6 us
    unnamed x27, local copies, waits for them, and re-layouts  24.9 us
    psum x1, blocking collectives, body(): energy = lax.psum(jnp.sum(direction * direction), ('fs', 'tp'))  16.5 us
    reduce_scatter x1, waiting for transfers between devices, body(): lax.psum_scatter(proj_rows, 'tp', scatter_dimension=1, tiled=True)  9.34 us
    dot_general x2, matrix products, split_product(): lax.dot_general(narrow, lower, numbers, preferred_element_type=jnp.float32)  8.03 us
    mul x1, local copies, waits for them, and re-layouts, head_output(): grouped * grouped  5.15 us
  transfers between devices with their start and end apart: 4, of which 4 were waited for; matrix products, arithmetic and copies ran while one was open for 6% of the time, Pallas kernels for 0%

commit v1 on v0

--- a/solution.py
+++ b/solution.py
@@ -1,8 +1,15 @@
+import functools
+
 import jax
 import jax.numpy as jnp
 from jax import lax
+from jax.experimental import pallas as pl
+from jax.experimental.pallas import tpu as pltpu
 from jax.sharding import PartitionSpec as P
 
+MESH = pl.DeviceIdType.MESH
+
+vmem_grant = 67043328
 out_scale = 0.8
 beta_first = 0.9
 beta_second = 0.95
@@ -64,9 +71,533 @@
     return (weight_new, weight_copy, step_out, first_new, second_new)
 
 
+def exchange_kernel(
+    axes,
+    lambda_ref,
+    gain_ref,
+    first_hbm,
+    second_hbm,
+    cot_hbm,
+    basis_hbm,
+    weight_hbm,
+    moment1_hbm,
+    moment2_hbm,
+    gathered_out,
+    direction_out,
+    projected_out,
+    first_v,
+    second_v,
+    cot_v,
+    basis_v,
+    weight_v,
+    narrow_v,
+    moment1_v,
+    moment2_v,
+    turned_v,
+    mine_v,
+    pair_send_v,
+    pair_recv_v,
+    plane_send_v,
+    plane_recv_v,
+    total_v,
+    line_send_v,
+    line_recv_v,
+    projected_v,
+    direction_v,
+    load_sem,
+    tile_sem,
+    wz_send,
+    wz_recv,
+    wp_send,
+    wp_recv,
+    pair_send,
+    pair_recv,
+    plane_send,
+    plane_recv,
+    line_send,
+    line_recv,
+    proj_send,
+    proj_recv,
+    dz_send,
+    dz_recv,
+    dp_send,
+    dp_recv,
+    dt_send,
+    dt_recv,
+):
+    line, plane = axes
+    fs, rep, tp = lax.axis_index("fs"), lax.axis_index("rep"), lax.axis_index("tp")
+    other = 1 - tp
+    tokens, width = cot_v.shape
+    half = direction_v.shape[-1]
+    quarter = direction_v.shape[-2]
+    shard = weight_v.shape[1]
+    weight_rows = weight_v.shape[0]
+    head_width = gain_ref.shape[1]
+    heads = first_v.shape[1] // head_width
+    tiles = tile_sem.shape[0]
+    tile = tokens // tiles
+
+    def ahead(at, step, count):
+        return lax.rem(at + 1 + step, count)
+
+    def behind(at, step, count):
+        return lax.rem(at + count - 1 - step, count)
+
+    def remote(source, target, send, recv, where):
+        return pltpu.make_async_remote_copy(
+            src_ref=source,
+            dst_ref=target,
+            send_sem=send,
+            recv_sem=recv,
+            device_id=where,
+            device_id_type=MESH,
+        )
+
+    my_rows = pl.ds(pl.multiple_of(rep * weight_rows, weight_rows), weight_rows)
+    my_quarter = pl.ds(pl.multiple_of(rep * quarter, quarter), quarter)
+
+    loads = [
+        pltpu.make_async_copy(weight_hbm.at[my_rows], weight_v, load_sem.at[0]),
+        pltpu.make_async_copy(
+            basis_hbm.at[:, pl.ds(pl.multiple_of(tp * half, half), half)],
+            basis_v.at[:, pl.ds(0, half)],
+            load_sem.at[1],
+        ),
+        pltpu.make_async_copy(
+            basis_hbm.at[:, pl.ds(pl.multiple_of(other * half, half), half)],
+            basis_v.at[:, pl.ds(half, half)],
+            load_sem.at[2],
+        ),
+        pltpu.make_async_copy(cot_hbm, cot_v, load_sem.at[3]),
+        pltpu.make_async_copy(moment1_hbm.at[my_quarter], moment1_v, load_sem.at[4]),
+        pltpu.make_async_copy(moment2_hbm.at[my_quarter], moment2_v, load_sem.at[5]),
+    ]
+    loads[0].start()
+    loads[1].start()
+    loads[2].start()
+    tile_loads = []
+    for t in range(tiles):
+        rows = pl.ds(t * tile, tile)
+        pieces = (
+            pltpu.make_async_copy(first_hbm.at[rows], first_v.at[rows], tile_sem.at[t, 0]),
+            pltpu.make_async_copy(second_hbm.at[rows], second_v.at[rows], tile_sem.at[t, 1]),
+        )
+        for piece in pieces:
+            piece.start()
+        tile_loads.append(pieces)
+    for load in loads[3:]:
+        load.start()
+
+    barrier = pltpu.get_barrier_semaphore()
+    for step in range(line - 1):
+        pl.semaphore_signal(
+            barrier, inc=1, device_id={"fs": ahead(fs, step, line)}, device_id_type=MESH
+        )
+    for step in range(plane - 1):
+        pl.semaphore_signal(
+            barrier, inc=1, device_id={"rep": ahead(rep, step, plane)}, device_id_type=MESH
+        )
+    pl.semaphore_signal(barrier, inc=1, device_id={"tp": other}, device_id_type=MESH)
+    pl.semaphore_wait(barrier, line + plane - 1)
+
+    sends = []
+    receives = []
+
+    loads[0].wait()
+    narrow_v[...] = weight_v[...].astype(jnp.bfloat16)
+    weight_line = []
+    for step in range(line - 1):
+        copy = remote(
+            narrow_v,
+            gathered_out.at[fs, my_rows],
+            wz_send.at[step],
+            wz_recv.at[step],
+            {"fs": ahead(fs, step, line)},
+        )
+        copy.start()
+        weight_line.append(copy)
+        sends.append(copy)
+
+    def pass_on(step):
+        weight_line[step].wait_recv()
+        source = behind(fs, step, line)
+        for to in range(plane - 1):
+            copy = remote(
+                gathered_out.at[source, my_rows],
+                gathered_out.at[source, my_rows],
+                wp_send.at[step, to],
+                wp_recv.at[step, to],
+                {"rep": ahead(rep, to, plane)},
+            )
+            copy.start()
+            sends.append(copy)
+            receives.append(copy)
+
+    loads[1].wait()
+    loads[2].wait()
+    gain = gain_ref[...] * out_scale
+    for t in range(tiles):
+        for piece in tile_loads[t]:
+            piece.wait()
+        rows = pl.ds(t * tile, tile)
+        reduced = None
+        for h in range(heads):
+            lanes = pl.ds(h * head_width, head_width)
+            mixture = first_v[rows, lanes].astype(jnp.float32) - lambda_ref[h] * second_v[
+                rows, lanes
+            ].astype(jnp.float32)
+            inverse = lax.rsqrt(jnp.mean(mixture * mixture, axis=-1, keepdims=True) + 1e-06)
+            normed = (mixture * inverse * gain).astype(jnp.bfloat16)
+            term = jnp.dot(normed, basis_v[lanes, :], preferred_element_type=jnp.float32)
+            reduced = term if reduced is None else reduced + term
+        turned_v[:, rows] = reduced.T.astype(jnp.bfloat16)
+
+    loads[3].wait()
+    pair_copies = []
+    plane_copies = []
+
+    def pair_sum(step):
+        pair_copies[step].wait_recv()
+        return mine_v[step] + pair_recv_v[step]
+
+    def send_plane(step):
+        plane_send_v[step] = pair_sum(step).astype(jnp.bfloat16)
+        copy = remote(
+            plane_send_v.at[step],
+            plane_recv_v.at[step],
+            plane_send.at[step],
+            plane_recv.at[step],
+            {"rep": ahead(rep, step, plane)},
+        )
+        copy.start()
+        plane_copies.append(copy)
+        sends.append(copy)
+
+    for step in range(plane):
+        part = ahead(rep, step, plane)
+        for at in range(line):
+            start = pl.multiple_of(at * shard + part * quarter, quarter)
+            product = jnp.dot(
+                turned_v[...], cot_v[:, pl.ds(start, quarter)], preferred_element_type=jnp.float32
+            )
+            mine_v[step, at] = product[:half].T
+            pair_send_v[step, at] = product[half:].T
+        copy = remote(
+            pair_send_v.at[step],
+            pair_recv_v.at[step],
+            pair_send.at[step],
+            pair_recv.at[step],
+            {"tp": other},
+        )
+        copy.start()
+        pair_copies.append(copy)
+        sends.append(copy)
+        if step > 0:
+            send_plane(step - 1)
+
+    pass_on(0)
+    total = pair_sum(plane - 1)
+    for step in range(plane - 1):
+        plane_copies[step].wait_recv()
+        total = total + plane_recv_v[step].astype(jnp.float32)
+    total_v[...] = total
+    line_send_v[...] = total.astype(jnp.bfloat16)
+    line_copies = []
+    for step in range(line - 1):
+        to = ahead(fs, step, line)
+        copy = remote(
+            line_send_v.at[to],
+            line_recv_v.at[step],
+            line_send.at[step],
+            line_recv.at[step],
+            {"fs": to},
+        )
+        copy.start()
+        line_copies.append(copy)
+        sends.append(copy)
+    for step in range(1, line - 2):
+        pass_on(step)
+    projected = total_v[fs]
+    for step in range(line - 1):
+        line_copies[step].wait_recv()
+        projected = projected + line_recv_v[step].astype(jnp.float32)
+    projected_v[rep] = projected
+    loads[4].wait()
+    loads[5].wait()
+    first_new = beta_first * moment1_v[...] + (1.0 - beta_first) * projected
+    second_new = beta_second * moment2_v[...] + (1.0 - beta_second) * projected * projected
+    direction = first_new / (jnp.sqrt(second_new) + 1e-08)
+    direction_v[tp, fs, rep] = direction.astype(jnp.bfloat16)
+    direction_line = []
+    for step in range(line - 1):
+        here = direction_v.at[tp, fs, rep]
+        copy = remote(
+            here, here, dz_send.at[step], dz_recv.at[step], {"fs": ahead(fs, step, line)}
+        )
+        copy.start()
+        direction_line.append(copy)
+        sends.append(copy)
+    for step in range(plane - 1):
+        here = projected_v.at[rep]
+        copy = remote(
+            here, here, proj_send.at[step], proj_recv.at[step], {"rep": ahead(rep, step, plane)}
+        )
+        copy.start()
+        sends.append(copy)
+        receives.append(copy)
+    for step in range(max(1, line - 2), line - 1):
+        pass_on(step)
+    for copy in direction_line:
+        copy.wait_recv()
+    direction_plane = []
+    for step in range(plane - 1):
+        here = direction_v.at[tp, :, rep]
+        copy = remote(
+            here, here, dp_send.at[step], dp_recv.at[step], {"rep": ahead(rep, step, plane)}
+        )
+        copy.start()
+        direction_plane.append(copy)
+        sends.append(copy)
+
+    def to_pair(step, part):
+        here = direction_v.at[tp, :, part]
+        copy = remote(here, here, dt_send.at[step], dt_recv.at[step], {"tp": other})
+        copy.start()
+        sends.append(copy)
+        receives.append(copy)
+
+    to_pair(plane - 1, rep)
+    for step in range(plane - 1):
+        direction_plane[step].wait_recv()
+        to_pair(step, behind(rep, step, plane))
+    for copy in receives:
+        copy.wait_recv()
+    outs = [
+        pltpu.make_async_copy(direction_v, direction_out, load_sem.at[0]),
+        pltpu.make_async_copy(projected_v, projected_out, load_sem.at[1]),
+    ]
+    for copy in outs:
+        copy.start()
+    for copy in sends:
+        copy.wait_send()
+    for copy in outs:
+        copy.wait()
+
+
+def update_kernel(
+    line,
+    basis_ref,
+    direction_ref,
+    projected_ref,
+    moment1_ref,
+    moment2_ref,
+    weight_ref,
+    gathered_ref,
+    weight_new_ref,
+    copy_ref,
+    step_ref,
+    first_new_ref,
+    second_new_ref,
+    scale_ref,
+    joined_ref,
+):
+    fs = lax.axis_index("fs")
+    shard = weight_ref.shape[1]
+
+    @pl.when(pl.program_id(0) == 0)
+    def _():
+        projected = projected_ref[...]
+        first_new_ref[...] = beta_first * moment1_ref[...] + (1.0 - beta_first) * projected
+        second_new_ref[...] = (
+            beta_second * moment2_ref[...] + (1.0 - beta_second) * projected * projected
+        )
+        half = direction_ref.shape[-1]
+        energy = jnp.zeros((1, half), jnp.float32)
+        for side in range(direction_ref.shape[0]):
+            piece = direction_ref[side]
+            joined_ref[:, side * half : (side + 1) * half] = piece
+            wide = piece.astype(jnp.float32)
+            energy += jnp.sum(wide * wide, axis=0, keepdims=True)
+        entries = joined_ref.shape[0] * joined_ref.shape[1]
+        spread = jnp.sqrt(jnp.sum(energy, axis=1, keepdims=True) / entries)
+        scale_ref[...] = jnp.broadcast_to(-1.0 / (spread + 1e-06), scale_ref.shape)
+
+    scale = scale_ref[0:1, 0:1]
+    basis = basis_ref[...]
+    for at in range(line):
+        columns = pl.ds(at * shard, shard)
+        step = (
+            lax.dot_general(
+                basis,
+                joined_ref[columns, :],
+                (((1,), (1,)), ((), ())),
+                preferred_element_type=jnp.float32,
+            )
+            * scale
+        )
+
+        @pl.when(fs == at)
+        def _():
+            fresh = weight_ref[...] + step
+            step_ref[...] = step
+            weight_new_ref[...] = fresh
+            copy_ref[:, columns] = fresh.astype(jnp.bfloat16)
+
+        @pl.when(fs != at)
+        def _():
+            copy_ref[:, columns] = (gathered_ref[at].astype(jnp.float32) + step).astype(
+                jnp.bfloat16
+            )
+
+
+def fast_body(
+    sizes,
+    first_mix,
+    second_mix,
+    lambda_head,
+    head_gain,
+    out_cotangent,
+    basis,
+    weight,
+    first_moment,
+    second_moment,
+):
+    line, plane = sizes
+    tokens, width = out_cotangent.shape
+    values, rank = basis.shape
+    shard, half = first_moment.shape
+    quarter = shard // plane
+    rows = values // plane
+    tile = 256 if tokens % 256 == 0 else tokens
+    tiles = tokens // tile
+    any_space = pl.BlockSpec(memory_space=pl.ANY)
+    dma = pltpu.SemaphoreType.DMA
+    f32, bf16 = jnp.float32, jnp.bfloat16
+    gathered, direction, projected = pl.pallas_call(
+        functools.partial(exchange_kernel, sizes),
+        out_shape=(
+            jax.ShapeDtypeStruct((line, values, shard), bf16),
+            jax.ShapeDtypeStruct((2, line, plane, quarter, half), bf16),
+            jax.ShapeDtypeStruct((plane, quarter, half), f32),
+        ),
+        in_specs=[
+            pl.BlockSpec(memory_space=pltpu.SMEM),
+            pl.BlockSpec(memory_space=pltpu.VMEM),
+        ]
+        + [any_space] * 7,
+        out_specs=(any_space,) * 3,
+        scratch_shapes=[
+            pltpu.VMEM(first_mix.shape, bf16),
+            pltpu.VMEM(second_mix.shape, bf16),
+            pltpu.VMEM(out_cotangent.shape, bf16),
+            pltpu.VMEM(basis.shape, bf16),
+            pltpu.VMEM((rows, shard), f32),
+            pltpu.VMEM((rows, shard), bf16),
+            pltpu.VMEM((quarter, half), f32),
+            pltpu.VMEM((quarter, half), f32),
+            pltpu.VMEM((rank, tokens), bf16),
+            pltpu.VMEM((plane, line, quarter, half), f32),
+            pltpu.VMEM((plane, line, quarter, half), f32),
+            pltpu.VMEM((plane, line, quarter, half), f32),
+            pltpu.VMEM((plane - 1, line, quarter, half), bf16),
+            pltpu.VMEM((plane - 1, line, quarter, half), bf16),
+            pltpu.VMEM((line, quarter, half), f32),
+            pltpu.VMEM((line, quarter, half), bf16),
+            pltpu.VMEM((line - 1, quarter, half), bf16),
+            pltpu.VMEM((plane, quarter, half), f32),
+            pltpu.VMEM((2, line, plane, quarter, half), bf16),
+            dma((6,)),
+            dma((tiles, 2)),
+            dma((line - 1,)),
+            dma((line - 1,)),
+            dma((line - 1, plane - 1)),
+            dma((line - 1, plane - 1)),
+            dma((plane,)),
+            dma((plane,)),
+            dma((plane - 1,)),
+            dma((plane - 1,)),
+            dma((line - 1,)),
+            dma((line - 1,)),
+            dma((plane - 1,)),
+            dma((plane - 1,)),
+            dma((line - 1,)),
+            dma((line - 1,)),
+            dma((plane - 1,)),
+            dma((plane - 1,)),
+            dma((plane,)),
+            dma((plane,)),
+        ],
+        compiler_params=pltpu.CompilerParams(
+            collective_id=0, has_side_effects=True, vmem_limit_bytes=vmem_grant
+        ),
+    )(
+        lambda_head,
+        head_gain.reshape(1, -1),
+        first_mix,
+        second_mix,
+        out_cotangent,
+        basis,
+        weight,
+        first_moment,
+        second_moment,
+    )
+    block = values // 4
+    whole = lambda *shape: pl.BlockSpec(shape, lambda i: (0,) * len(shape))
+    rowed = lambda columns: pl.BlockSpec((block, columns), lambda i: (i, 0))
+    return pl.pallas_call(
+        functools.partial(update_kernel, line),
+        grid=(values // block,),
+        out_shape=(
+            jax.ShapeDtypeStruct(weight.shape, f32),
+            jax.ShapeDtypeStruct((values, width), bf16),
+            jax.ShapeDtypeStruct(weight.shape, f32),
+            jax.ShapeDtypeStruct(first_moment.shape, f32),
+            jax.ShapeDtypeStruct(first_moment.shape, f32),
+        ),
+        in_specs=[
+            rowed(rank),
+            whole(2, width, half),
+            whole(shard, half),
+            whole(shard, half),
+            whole(shard, half),
+            rowed(shard),
+            pl.BlockSpec((line, block, shard), lambda i: (0, i, 0)),
+        ],
+        out_specs=(
+            rowed(shard),
+            rowed(width),
+            rowed(shard),
+            whole(shard, half),
+            whole(shard, half),
+        ),
+        scratch_shapes=[pltpu.VMEM((8, 128), f32), pltpu.VMEM((width, rank), bf16)],
+        compiler_params=pltpu.CompilerParams(vmem_limit_bytes=vmem_grant),
+    )(
+        basis,
+        direction.reshape(2, width, half),
+        projected.reshape(shard, half),
+        first_moment,
+        second_moment,
+        weight,
+        gathered,
+    )
+
+
 def solution(mesh):
+    line, plane, pair = (mesh.shape[name] for name in ("fs", "rep", "tp"))
+
+    def chosen(*args):
+        basis, first_moment = args[5], args[7]
+        quarter_fits = first_moment.shape[0] % (plane * 128) == 0
+        rows_fit = basis.shape[0] % (plane * 16) == 0 and basis.shape[0] % 64 == 0
+        rank_fits = pair == 2 and first_moment.shape[1] % 128 == 0
+        if min(line, plane) > 1 and quarter_fits and rows_fit and rank_fits:
+            return fast_body((line, plane), *args)
+        return body(*args)
+
     return jax.shard_map(
-        body,
+        chosen,
         mesh=mesh,
         in_specs=(
             P(("fs", "rep"), "tp"),

time: 255 us -> 75.4 us (0.30)
  waiting for transfers between devices: 167 us -> 0 us
  Pallas kernels: 0 us -> 73.7 us
  local copies, waits for them, and re-layouts: 31 us -> 0 us
  blocking collectives: 18.7 us -> 0 us
  between operations: 14.6 us -> 0.64 us
  matrix products: 12.8 us -> 0 us
  other arithmetic: 9.72 us -> 0 us
    pallas_call x0 -> x2, Pallas kernels: none -> 73.7 us  [the longest x1 63.3 us: fast_body(): pl.pallas_call(functools.partial(exchange_kernel, sizes), out_shape=(jax....]
    all_gather x1 -> x0, waiting for transfers between devices: 69.5 us -> none  [body(): lax.all_gather(weight_new.astype(jnp.bfloat16), 'fs', axis=1, tiled=True)]
    reduce_scatter x2 -> x0, waiting for transfers between devices: 55.8 us -> none  [the longest x1 46.5 us: body(): lax.psum_scatter(split_product(out_cotangent, reduced, (((0,), (0,)), (()...]
    psum x1 -> x0, waiting for transfers between devices: 41.6 us -> none  [body(): projected = lax.psum(proj_rows, 'rep')]
    unnamed x27 -> x0, local copies, waits for them, and re-layouts: 24.9 us -> none
    psum x1 -> x0, blocking collectives: 16.5 us -> none  [body(): energy = lax.psum(jnp.sum(direction * direction), ('fs', 'tp'))]
    dot_general x5 -> x0, matrix products: 12.8 us -> none  [the longest x2 8.03 us: split_product(): lax.dot_general(narrow, lower, numbers, preferred_element_type=jnp.float32)]
    mul x2 -> x0, local copies, waits for them, and re-layouts: 6.13 us -> none  [the longest x1 5.15 us: head_output(): grouped * grouped]
  transfers between devices with their start and end apart: 4 -> 0, of which waited for: 4 -> 0; matrix products, arithmetic and copies ran while one was open for 6% -> 0% of each run, Pallas kernels for 0% -> 0%
where the time goes in v1:
time: 75.4 us; the launch traced here: 74.3 us
  Pallas kernels  73.7 us (98%)
    pallas_call x1, Pallas kernels, fast_body(): pl.pallas_call(functools.partial(exchange_kernel, sizes), out_shape=(jax....  63.3 us
    pallas_call x1, Pallas kernels, fast_body(): pl.pallas_call(functools.partial(update_kernel, line), grid=(values // bl...  10.4 us

profile of v1, /device:TPU:0, one launch (start us, length us, event | category | flops | bytes accessed | tf_op | source)
XLA Modules:
  0.0 74.3 jit_solution(3333478841059348261)
XLA Ops:
  0.6 63.3 %shard_map.128 = (bf16[4,1024,512]{2,1,0:T(8,128)(2,1)}, bf16[2,4,4,128,128]{4,3,2,1,0:T(8,128)(2,1)}, f32[4,128,128]{2,1,0:T(8,128)}) custom-call(f32[4]{0:T(128)} %lambda_ref.1, f32[1,256]{1,0:T(1,128)} %bitcast.5, bf16[768,1024]{1,0:T(8,128)(2,1)} %first_hbm.1, bf16[768,1024]{1,0:T(8,128)(2,1)} %second_hbm.1, bf16[768,2048]{1,0:T(8,128)(2,1)} %cot_hbm.1, ...), custom_call_target="tpu_custom_call" | custom-call | tf_op jit(solution)/shard_map/pallas_call | solution.py:477
  63.9 10.4 %shard_map.129 = (f32[1024,512]{1,0:T(8,128)}, bf16[1024,2048]{1,0:T(8,128)(2,1)}, f32[1024,512]{1,0:T(8,128)}, f32[512,128]{1,0:T(8,128)}, f32[512,128]{1,0:T(8,128)}) custom-call(bf16[1024,256]{1,0:T(8,128)(2,1)} %basis_ref.1, bf16[2,2048,128]{2,1,0:T(8,128)(2,1)} %bitcast.3, f32[512,128]{1,0:T(8,128)} %bitcast.4, f32[512,128]{1,0:T(8,128)} %moment1_ref.1, ...), custom_call_target="tpu_custom_call" | custom-call | tf_op jit(solution)/shard_map/pallas_call | solution.py:548

commit v2 on v1

--- a/solution.py
+++ b/solution.py
@@ -85,6 +85,7 @@
     gathered_out,
     direction_out,
     projected_out,
+    scale_out,
     first_v,
     second_v,
     cot_v,
@@ -104,6 +105,8 @@
     line_recv_v,
     projected_v,
     direction_v,
+    joined_v,
+    scale_v,
     load_sem,
     tile_sem,
     wz_send,
@@ -144,6 +147,10 @@
     def behind(at, step, count):
         return lax.rem(at + count - 1 - step, count)
 
+    fast_side = rep + 1 - 2 * lax.rem(rep, 2)
+    slow_side = lax.rem(rep + 2, 4)
+    peers = (3 - rep, slow_side, fast_side, rep)
+
     def remote(source, target, send, recv, where):
         return pltpu.make_async_remote_copy(
             src_ref=source,
@@ -196,18 +203,21 @@
         )
     for step in range(plane - 1):
         pl.semaphore_signal(
-            barrier, inc=1, device_id={"rep": ahead(rep, step, plane)}, device_id_type=MESH
+            barrier, inc=1, device_id={"rep": peers[step]}, device_id_type=MESH
         )
     pl.semaphore_signal(barrier, inc=1, device_id={"tp": other}, device_id_type=MESH)
     pl.semaphore_wait(barrier, line + plane - 1)
 
     sends = []
     receives = []
+    pair_receives = []
+    proj_receives = []
 
     loads[0].wait()
     narrow_v[...] = weight_v[...].astype(jnp.bfloat16)
-    weight_line = []
-    for step in range(line - 1):
+    weight_line = {}
+
+    def send_line(step):
         copy = remote(
             narrow_v,
             gathered_out.at[fs, my_rows],
@@ -216,19 +226,36 @@
             {"fs": ahead(fs, step, line)},
         )
         copy.start()
-        weight_line.append(copy)
-        sends.append(copy)
+        weight_line[step] = copy
+        sends.append(copy)
+
+    early = (0, line - 2)
+    late = tuple(range(1, line - 2))
+    for step in early:
+        send_line(step)
+
+    side_copies = {}
 
     def pass_on(step):
         weight_line[step].wait_recv()
+        here = gathered_out.at[behind(fs, step, line), my_rows]
+        for side, peer in enumerate((slow_side, fast_side)):
+            copy = remote(
+                here, here, wp_send.at[step, side], wp_recv.at[step, side], {"rep": peer}
+            )
+            copy.start()
+            sends.append(copy)
+            side_copies[step, side] = copy
+
+    def relay(step):
         source = behind(fs, step, line)
-        for to in range(plane - 1):
+        part = weight_rows // 2
+        for side, (origin, peer) in enumerate(((slow_side, fast_side), (fast_side, slow_side))):
+            side_copies[step, side].wait_recv()
+            start = pl.multiple_of(origin * weight_rows + side * part, part)
+            here = gathered_out.at[source, pl.ds(start, part)]
             copy = remote(
-                gathered_out.at[source, my_rows],
-                gathered_out.at[source, my_rows],
-                wp_send.at[step, to],
-                wp_recv.at[step, to],
-                {"rep": ahead(rep, to, plane)},
+                here, here, wp_send.at[step, 2 + side], wp_recv.at[step, 2 + side], {"rep": peer}
             )
             copy.start()
             sends.append(copy)
@@ -268,14 +295,14 @@
             plane_recv_v.at[step],
             plane_send.at[step],
             plane_recv.at[step],
-            {"rep": ahead(rep, step, plane)},
+            {"rep": peers[step]},
         )
         copy.start()
         plane_copies.append(copy)
         sends.append(copy)
 
     for step in range(plane):
-        part = ahead(rep, step, plane)
+        part = peers[step]
         for at in range(line):
             start = pl.multiple_of(at * shard + part * quarter, quarter)
             product = jnp.dot(
@@ -316,8 +343,8 @@
         copy.start()
         line_copies.append(copy)
         sends.append(copy)
-    for step in range(1, line - 2):
-        pass_on(step)
+    relay(0)
+    pass_on(line - 2)
     projected = total_v[fs]
     for step in range(line - 1):
         line_copies[step].wait_recv()
@@ -338,23 +365,23 @@
         copy.start()
         direction_line.append(copy)
         sends.append(copy)
+    for step in late:
+        send_line(step)
     for step in range(plane - 1):
         here = projected_v.at[rep]
         copy = remote(
-            here, here, proj_send.at[step], proj_recv.at[step], {"rep": ahead(rep, step, plane)}
-        )
-        copy.start()
-        sends.append(copy)
-        receives.append(copy)
-    for step in range(max(1, line - 2), line - 1):
-        pass_on(step)
+            here, here, proj_send.at[step], proj_recv.at[step], {"rep": peers[step]}
+        )
+        copy.start()
+        sends.append(copy)
+        proj_receives.append(copy)
     for copy in direction_line:
         copy.wait_recv()
     direction_plane = []
     for step in range(plane - 1):
         here = direction_v.at[tp, :, rep]
         copy = remote(
-            here, here, dp_send.at[step], dp_recv.at[step], {"rep": ahead(rep, step, plane)}
+            here, here, dp_send.at[step], dp_recv.at[step], {"rep": peers[step]}
         )
         copy.start()
         direction_plane.append(copy)
@@ -365,20 +392,38 @@
         copy = remote(here, here, dt_send.at[step], dt_recv.at[step], {"tp": other})
         copy.start()
         sends.append(copy)
-        receives.append(copy)
+        pair_receives.append(copy)
 
     to_pair(plane - 1, rep)
     for step in range(plane - 1):
         direction_plane[step].wait_recv()
-        to_pair(step, behind(rep, step, plane))
+        to_pair(step, peers[step])
+    relay(line - 2)
+    for step in late:
+        pass_on(step)
+    for copy in pair_receives:
+        copy.wait_recv()
+    energy = jnp.zeros((1, half), jnp.float32)
+    for side in range(2):
+        piece = direction_v[side].reshape(width, half)
+        wide = piece.astype(jnp.float32)
+        joined_v[side * half : (side + 1) * half, :] = wide.T.astype(jnp.bfloat16)
+        energy += jnp.sum(wide * wide, axis=0, keepdims=True)
+    spread = jnp.sqrt(jnp.sum(energy, axis=1, keepdims=True) / (width * 2 * half))
+    scale_v[...] = jnp.broadcast_to(-1.0 / (spread + 1e-06), scale_v.shape)
+    for step in late:
+        relay(step)
+    for copy in proj_receives:
+        copy.wait_recv()
+    outs = [
+        pltpu.make_async_copy(joined_v, direction_out, load_sem.at[0]),
+        pltpu.make_async_copy(projected_v, projected_out, load_sem.at[1]),
+        pltpu.make_async_copy(scale_v, scale_out, load_sem.at[2]),
+    ]
+    for copy in outs:
+        copy.start()
     for copy in receives:
         copy.wait_recv()
-    outs = [
-        pltpu.make_async_copy(direction_v, direction_out, load_sem.at[0]),
-        pltpu.make_async_copy(projected_v, projected_out, load_sem.at[1]),
-    ]
-    for copy in outs:
-        copy.start()
     for copy in sends:
         copy.wait_send()
     for copy in outs:
@@ -389,6 +434,7 @@
     line,
     basis_ref,
     direction_ref,
+    scale_ref,
     projected_ref,
     moment1_ref,
     moment2_ref,
@@ -399,41 +445,20 @@
     step_ref,
     first_new_ref,
     second_new_ref,
-    scale_ref,
-    joined_ref,
 ):
     fs = lax.axis_index("fs")
     shard = weight_ref.shape[1]
-
-    @pl.when(pl.program_id(0) == 0)
-    def _():
-        projected = projected_ref[...]
-        first_new_ref[...] = beta_first * moment1_ref[...] + (1.0 - beta_first) * projected
-        second_new_ref[...] = (
-            beta_second * moment2_ref[...] + (1.0 - beta_second) * projected * projected
-        )
-        half = direction_ref.shape[-1]
-        energy = jnp.zeros((1, half), jnp.float32)
-        for side in range(direction_ref.shape[0]):
-            piece = direction_ref[side]
-            joined_ref[:, side * half : (side + 1) * half] = piece
-            wide = piece.astype(jnp.float32)
-            energy += jnp.sum(wide * wide, axis=0, keepdims=True)
-        entries = joined_ref.shape[0] * joined_ref.shape[1]
-        spread = jnp.sqrt(jnp.sum(energy, axis=1, keepdims=True) / entries)
-        scale_ref[...] = jnp.broadcast_to(-1.0 / (spread + 1e-06), scale_ref.shape)
-
+    projected = projected_ref[...]
+    first_new_ref[...] = beta_first * moment1_ref[...] + (1.0 - beta_first) * projected
+    second_new_ref[...] = (
+        beta_second * moment2_ref[...] + (1.0 - beta_second) * projected * projected
+    )
     scale = scale_ref[0:1, 0:1]
     basis = basis_ref[...]
     for at in range(line):
         columns = pl.ds(at * shard, shard)
         step = (
-            lax.dot_general(
-                basis,
-                joined_ref[columns, :],
-                (((1,), (1,)), ((), ())),
-                preferred_element_type=jnp.float32,
-            )
+            jnp.dot(basis, direction_ref[:, columns], preferred_element_type=jnp.float32)
             * scale
         )
 
@@ -474,19 +499,20 @@
     any_space = pl.BlockSpec(memory_space=pl.ANY)
     dma = pltpu.SemaphoreType.DMA
     f32, bf16 = jnp.float32, jnp.bfloat16
-    gathered, direction, projected = pl.pallas_call(
+    gathered, direction, projected, scale = pl.pallas_call(
         functools.partial(exchange_kernel, sizes),
         out_shape=(
             jax.ShapeDtypeStruct((line, values, shard), bf16),
-            jax.ShapeDtypeStruct((2, line, plane, quarter, half), bf16),
+            jax.ShapeDtypeStruct((rank, width), bf16),
             jax.ShapeDtypeStruct((plane, quarter, half), f32),
+            jax.ShapeDtypeStruct((8, 128), f32),
         ),
         in_specs=[
             pl.BlockSpec(memory_space=pltpu.SMEM),
             pl.BlockSpec(memory_space=pltpu.VMEM),
         ]
         + [any_space] * 7,
-        out_specs=(any_space,) * 3,
+        out_specs=(any_space,) * 4,
         scratch_shapes=[
             pltpu.VMEM(first_mix.shape, bf16),
             pltpu.VMEM(second_mix.shape, bf16),
@@ -507,12 +533,14 @@
             pltpu.VMEM((line - 1, quarter, half), bf16),
             pltpu.VMEM((plane, quarter, half), f32),
             pltpu.VMEM((2, line, plane, quarter, half), bf16),
+            pltpu.VMEM((rank, width), bf16),
+            pltpu.VMEM((8, 128), f32),
             dma((6,)),
             dma((tiles, 2)),
             dma((line - 1,)),
             dma((line - 1,)),
-            dma((line - 1, plane - 1)),
-            dma((line - 1, plane - 1)),
+            dma((line - 1, 4)),
+            dma((line - 1, 4)),
             dma((plane,)),
             dma((plane,)),
             dma((plane - 1,)),
@@ -542,8 +570,11 @@
         first_moment,
         second_moment,
     )
-    block = values // 4
+    blocks = 2
+    block = values // blocks
+    moment_block = shard // blocks
     whole = lambda *shape: pl.BlockSpec(shape, lambda i: (0,) * len(shape))
+    mrow = pl.BlockSpec((moment_block, half), lambda i: (i, 0))
     rowed = lambda columns: pl.BlockSpec((block, columns), lambda i: (i, 0))
     return pl.pallas_call(
         functools.partial(update_kernel, line),
@@ -557,10 +588,11 @@
         ),
         in_specs=[
             rowed(rank),
-            whole(2, width, half),
-            whole(shard, half),
-            whole(shard, half),
-            whole(shard, half),
+            whole(rank, width),
+            whole(8, 128),
+            mrow,
+            mrow,
+            mrow,
             rowed(shard),
             pl.BlockSpec((line, block, shard), lambda i: (0, i, 0)),
         ],
@@ -568,14 +600,14 @@
             rowed(shard),
             rowed(width),
             rowed(shard),
-            whole(shard, half),
-            whole(shard, half),
+            mrow,
+            mrow,
         ),
-        scratch_shapes=[pltpu.VMEM((8, 128), f32), pltpu.VMEM((width, rank), bf16)],
         compiler_params=pltpu.CompilerParams(vmem_limit_bytes=vmem_grant),
     )(
         basis,
-        direction.reshape(2, width, half),
+        direction,
+        scale,
         projected.reshape(shard, half),
         first_moment,
         second_moment,
@@ -592,7 +624,7 @@
         quarter_fits = first_moment.shape[0] % (plane * 128) == 0
         rows_fit = basis.shape[0] % (plane * 16) == 0 and basis.shape[0] % 64 == 0
         rank_fits = pair == 2 and first_moment.shape[1] % 128 == 0
-        if min(line, plane) > 1 and quarter_fits and rows_fit and rank_fits:
+        if line > 2 and plane == 4 and quarter_fits and rows_fit and rank_fits:
             return fast_body((line, plane), *args)
         return body(*args)
 

time: 75.4 us -> 66.9 us (0.89); the launches traced: 74.3 us -> 66.7 us
  Pallas kernels: 73.7 us -> 66.1 us
    pallas_call x1, Pallas kernels: 63.3 us -> 58.2 us  [fast_body(): pl.pallas_call(functools.partial(exchange_kernel, sizes), out_shape=(jax....]
    pallas_call x1, Pallas kernels: 10.4 us -> 7.92 us  [fast_body(): pl.pallas_call(functools.partial(update_kernel, line), grid=(values // bl...]
where the time goes in v2:
time: 66.9 us; the launch traced here: 66.7 us
  Pallas kernels  66.1 us (99%)
    pallas_call x1, Pallas kernels, fast_body(): pl.pallas_call(functools.partial(exchange_kernel, sizes), out_shape=(jax....  58.2 us
    pallas_call x1, Pallas kernels, fast_body(): pl.pallas_call(functools.partial(update_kernel, line), grid=(values // bl...  7.92 us

profile of v2, /device:TPU:0, one launch (start us, length us, event | category | flops | bytes accessed | tf_op | source)
XLA Modules:
  0.0 66.7 jit_solution(7215975111016463102)
XLA Ops:
  0.6 58.2 %shard_map.128 = (bf16[4,1024,512]{2,1,0:T(8,128)(2,1)}, bf16[256,2048]{1,0:T(8,128)(2,1)}, f32[4,128,128]{2,1,0:T(8,128)}, f32[8,128]{1,0:T(8,128)}) custom-call(f32[4]{0:T(128)} %lambda_ref.1, f32[1,256]{1,0:T(1,128)} %bitcast.3, bf16[768,1024]{1,0:T(8,128)(2,1)} %first_hbm.1, bf16[768,1024]{1,0:T(8,128)(2,1)} %second_hbm.1, bf16[768,2048]{1,0:T(8,128)(2,1)} %cot_hbm.1, ...), custom_call_target="tpu_custom_call" | custom-call | tf_op jit(solution)/shard_map/pallas_call | solution.py:502
  58.8 7.9 %shard_map.129 = (f32[1024,512]{1,0:T(8,128)}, bf16[1024,2048]{1,0:T(8,128)(2,1)}, f32[1024,512]{1,0:T(8,128)}, f32[512,128]{1,0:T(8,128)}, f32[512,128]{1,0:T(8,128)}) custom-call(bf16[1024,256]{1,0:T(8,128)(2,1)} %basis_ref.1, bf16[256,2048]{1,0:T(8,128)(2,1)} %get-tuple-element.9.direction_ref, f32[8,128]{1,0:T(8,128)} %get-tuple-element.10.scale_ref, ...), custom_call_target="tpu_custom_call" | custom-call | tf_op jit(solution)/shard_map/pallas_call | solution.py:579
